TPU v7x, 256 devices: a 4x2x16 block of a 4x16x16 slice. The times are simulated.
256 devices in a mesh: grp: 2 (over y), kv: 32 (over z, core), tp: 4 (over x).
Axes of the slice: x: 4, y: 2, z: 16, core: 2. Of those that a mesh axis runs over, the one named last changes fastest.
The devices are a block of a 4x16x16 slice.
Arguments:
- hidden: bfloat16 [2048, 4096], P('grp', 'kv'), parts along dimension 0, may hold values from -64 to 64
- norm_gain: bfloat16 [4096], replicated, may hold values from 0.099609375 to 1.8984375
- w_query: bfloat16 [4096, 2048], P('kv', 'tp'), may hold values from -0.09375 to 0.09375
- w_key: bfloat16 [4096, 2048], P('kv', 'tp'), may hold values from -0.09375 to 0.09375
- w_value: bfloat16 [4096, 2048], P('kv', 'tp'), may hold values from -0.09375 to 0.09375
- w_gate: bfloat16 [4096, 2048], P('kv', 'tp'), may hold values from -0.09375 to 0.09375
- w_decay: bfloat16 [4096, 16], P(None, 'tp'), may hold values from -0.09375 to 0.09375
- w_write: bfloat16 [4096, 16], P(None, 'tp'), may hold values from -0.09375 to 0.09375
- decay_rate: float32 [16], P('tp'), may hold values from 0.02 to 1
- head_gain: bfloat16 [128], replicated, may hold values from 0.099609375 to 1.8984375
- w_output: bfloat16 [2048, 4096], P('tp', 'kv'), may hold values from -0.125 to 0.125
- state: float32 [512, 16, 16384], P(('grp', 'kv'), 'tp'), parts along dimension 0, may hold values from -6 to 6
- prev_keys: bfloat16 [512, 4, 2048], P(('grp', 'kv'), None, 'tp'), parts along dimension 0, may hold values from -6 to 6
- prev_values: bfloat16 [512, 4, 2048], P(('grp', 'kv'), None, 'tp'), parts along dimension 0, may hold values from -6 to 6
- prev_decay: float32 [512, 4, 16], P(('grp', 'kv'), None, 'tp'), parts along dimension 0, may hold values from -1 to -0.02
- prev_write: float32 [512, 4, 16], P(('grp', 'kv'), None, 'tp'), parts along dimension 0, may hold values from 0.05 to 0.95
- accepted: int32 [512], P(('grp', 'kv')), parts along dimension 0, may hold values from 0 to 4
Outputs:
- mixed: bfloat16 [2048, 4096], P('grp', 'kv'), parts along dimension 0
- state_out: float32 [512, 16, 16384], P(('grp', 'kv'), 'tp'), parts along dimension 0
There are 2 independent parts, one for each index of `grp`. A program takes and returns all parts, laid end to end along the dimension named above; an argument that names none is the same for every part. Nothing has to cross between parts.
All inputs are finite; a program needn't handle non-finite values.
Results may differ from a plain program's by a relative error of at most 0.0069.
Values may be sent and summed in bfloat16 or wider, within the bound.
A program may use at most 64 MiB of HBM per device.

v0:
```python
import jax
import jax.numpy as jnp
from jax import lax
from jax.sharding import Mesh
from jax.sharding import PartitionSpec as P

KV = ("kv_0", "kv_1")
GRP_KV = ("grp", "kv_0", "kv_1")
EPSILON = 1e-06


def side_by_side(arrays, axis, dim, along):
    ends, at = ([], 0)
    for a in arrays[:-1]:
        at += a.shape[along]
        ends.append(at)
    both = jnp.concatenate(arrays, axis=along)
    return tuple(jnp.split(lax.all_gather(both, axis, axis=dim, tiled=True), ends, axis=along))


def in_order(tiles, dim):
    tiles = jnp.moveaxis(tiles, 0, dim)
    shape = tiles.shape
    return tiles.reshape(*shape[:dim], shape[dim] * shape[dim + 1], *shape[dim + 2 :])


def gather_in_order(value, axes, turns):
    tiles = value[None]
    for k in turns:
        tiles = lax.all_gather(tiles, axes[k], axis=0, tiled=True)
    block = [lax.axis_size(axes[k]) for k in reversed(turns)]
    tiles = tiles.reshape(*block, *value.shape)
    turned = sorted(range(len(turns)), key=lambda place: turns[len(turns) - 1 - place])
    return tiles.transpose(*turned, *range(len(turns), tiles.ndim)).reshape(-1, *value.shape)


def whole_of(value, axes, turns, dim):
    return in_order(gather_in_order(value, axes, turns), dim)


def from_everyone(value, axis):
    copies = jnp.broadcast_to(value, (lax.axis_size(axis), *value.shape))
    return lax.all_to_all(copies, axis, split_axis=0, concat_axis=0, tiled=True)


def of_everyone(value, axis):
    return from_everyone(value, axis).sum(axis=0)


def unit_rows(values):
    return values * lax.rsqrt(jnp.sum(values * values, axis=-1, keepdims=True) + EPSILON)


def delta_block(carried_state, keys, values, log_decay, writes, query_rows):
    length = keys.shape[2]
    totals = jnp.cumsum(log_decay, axis=-1)
    spread = totals[..., :, None] - totals[..., None, :]
    lower = jnp.tril(jnp.ones((length, length), dtype=bool))
    strict = jnp.tril(jnp.ones((length, length), dtype=bool), -1)
    within = jnp.where(lower, jnp.exp(jnp.where(lower, spread, 0.0)), 0.0)
    affinity = jnp.einsum("shid,shjd->shij", keys, keys, precision=lax.Precision.HIGHEST)
    coupling = jnp.where(strict, writes[..., :, None] * affinity * within, 0.0)
    source = jnp.concatenate(
        [values * writes[..., None], keys * (writes * jnp.exp(totals))[..., None]], axis=-1
    )
    solved = []
    for token_position in range(length):
        current = source[:, :, token_position]
        for earlier in range(token_position):
            current = current - coupling[:, :, token_position, earlier][..., None] * solved[earlier]
        solved.append(current)
    solved = jnp.stack(solved, axis=2)
    head_size = keys.shape[-1]
    fresh = solved[..., :head_size] - jnp.einsum(
        "shpk,shkv->shpv", solved[..., head_size:], carried_state, precision=lax.Precision.HIGHEST
    )
    outputs = None
    if query_rows is not None:
        scores = (
            jnp.einsum("shid,shjd->shij", query_rows, keys, precision=lax.Precision.HIGHEST)
            * within
        )
        outputs = jnp.einsum(
            "shpk,shkv->shpv",
            query_rows * jnp.exp(totals)[..., None],
            carried_state,
            precision=lax.Precision.HIGHEST,
        )
        outputs = outputs + jnp.einsum(
            "shij,shjv->shiv", scores, fresh, precision=lax.Precision.HIGHEST
        )
    final = totals[..., -1:]
    carried_state = carried_state * jnp.exp(final)[..., None] + jnp.einsum(
        "shpk,shpv->shkv",
        keys * jnp.exp(final - totals)[..., None],
        fresh,
        precision=lax.Precision.HIGHEST,
    )
    return (carried_state, outputs)


def per_device(
    hidden,
    norm_gain,
    w_query,
    w_key,
    w_value,
    w_gate,
    w_decay,
    w_write,
    decay_rate,
    head_gain,
    w_output,
    state,
    prev_keys,
    prev_values,
    prev_decay,
    prev_write,
    accepted,
):
    heads = w_decay.shape[1]
    width = w_query.shape[1]
    head_size = width // heads
    token_block = lax.all_to_all(hidden, KV, split_axis=0, concat_axis=1, tiled=True)
    wide = token_block.astype(jnp.float32)
    scaled = (wide * norm_gain.astype(jnp.float32)).astype(jnp.bfloat16)
    squares = jnp.sum(wide * wide, axis=1)
    pieces = side_by_side((w_query, w_key, w_value, w_gate), KV, 0, 1)
    summed = tuple((jnp.dot(scaled, piece, preferred_element_type=jnp.float32) for piece in pieces))
    projected = jnp.concatenate(summed, axis=1)
    small = jnp.dot(
        scaled, jnp.concatenate([w_decay, w_write], axis=1), preferred_element_type=jnp.float32
    )
    inverse = lax.rsqrt(squares / norm_gain.shape[0] + EPSILON)
    projected = projected * inverse[:, None]
    small = small * inverse[:, None]
    seqs = state.shape[0]
    proposals = projected.shape[0] // seqs

    def heads_first(block):
        return block.reshape(seqs, proposals, heads, head_size).transpose(0, 2, 1, 3)

    query_rows = unit_rows(heads_first(projected[:, :width])) * head_size ** (-0.5)
    keys = unit_rows(heads_first(projected[:, width : 2 * width]))
    values = heads_first(projected[:, 2 * width : 3 * width])
    gates = projected[:, 3 * width :].reshape(seqs, proposals, heads, head_size)
    log_decay = (
        (-decay_rate * jax.nn.softplus(small[:, :heads]))
        .reshape(seqs, proposals, heads)
        .transpose(0, 2, 1)
    )
    writes = jax.nn.sigmoid(small[:, heads:]).reshape(seqs, proposals, heads).transpose(0, 2, 1)
    taken = jnp.arange(proposals, dtype=jnp.int32)[None, :] < accepted[:, None]
    old_keys = unit_rows(
        prev_keys.astype(jnp.float32)
        .reshape(seqs, proposals, heads, head_size)
        .transpose(0, 2, 1, 3)
    )
    old_values = (
        prev_values.astype(jnp.float32)
        .reshape(seqs, proposals, heads, head_size)
        .transpose(0, 2, 1, 3)
    )
    old_decay = jnp.where(taken[:, :, None], prev_decay, 0.0).transpose(0, 2, 1)
    old_writes = jnp.where(taken[:, :, None], prev_write, 0.0).transpose(0, 2, 1)
    carried_state = state.reshape(seqs, heads, head_size, head_size)
    carried_state, _ = delta_block(carried_state, old_keys, old_values, old_decay, old_writes, None)
    _, outputs = delta_block(carried_state, keys, values, log_decay, writes, query_rows)
    outputs = outputs.transpose(0, 2, 1, 3)
    normed = outputs * lax.rsqrt(jnp.mean(outputs * outputs, axis=-1, keepdims=True) + EPSILON)
    normed = normed * head_gain.astype(jnp.float32) * jax.nn.silu(gates)
    heads_out = normed.reshape(seqs * proposals, width).astype(jnp.bfloat16)
    terms = jnp.dot(
        whole_of(heads_out, KV, (0, 1), 0), w_output, preferred_element_type=jnp.float32
    )
    mixed = of_everyone(terms, "tp").astype(jnp.bfloat16)
    return (mixed, carried_state.reshape(seqs, heads, head_size * head_size))


def solution(mesh):
    torus = Mesh(
        mesh.devices.reshape(mesh.shape["grp"], 16, 2, mesh.shape["tp"]),
        ("grp", "kv_0", "kv_1", "tp"),
    )
    in_specs = (
        P("grp", KV),
        P(),
        P(KV, "tp"),
        P(KV, "tp"),
        P(KV, "tp"),
        P(KV, "tp"),
        P(None, "tp"),
        P(None, "tp"),
        P("tp"),
        P(),
        P("tp", KV),
        P(GRP_KV, "tp", None),
        P(GRP_KV, None, "tp"),
        P(GRP_KV, None, "tp"),
        P(GRP_KV, None, "tp"),
        P(GRP_KV, None, "tp"),
        P(GRP_KV),
    )
    out_specs = (P("grp", KV), P(GRP_KV, "tp", None))
    return jax.shard_map(
        per_device, mesh=torus, in_specs=in_specs, out_specs=out_specs, check_vma=False
    )
```

profile of v0, /device:TPU:33, one launch (start us, length us, event | category | flops | bytes accessed | tf_op | source)
XLA Modules:
  0.0 251.3 jit_solution(17397073867392320041)
XLA Ops:
  7.3 2.0 pad_maximum_fusion
  9.4 25.5 %all-to-all-start = ((bf16[32,32,128]{2,1,0:T(8,128)(2,1)}), bf16[32,32,128]{2,1,0:T(8,128)(2,1)S(1)}, u32[]{:S(2)}, u32[]{:S(2)}) async-start(bf16[32,32,128]{2,1,0:T(8,128)(2,1)} %bitcast.155), calls=%async_computation | async-start | bytes 524288 | tf_op jit(solution)/shard_map/all_to_all | solution.py:124
  35.0 0.1 copy.357
  35.2 0.1 copy.354
  35.3 0.1 copy.355
  35.4 0.1 fusion.31
  35.6 0.4 fusion.11
  36.1 0.2 fusion.19
  36.2 0.2 fusion.79
  36.5 2.7 %reshape.141 = f32[8,4,128,128]{3,2,1,0:T(8,128)S(1)} reshape(f32[8,4,16384]{2,1,0:T(4,128)} %param.28) | data formatting | bytes 4194304 | tf_op jit(solution)/shard_map/reshape | solution.py:166
  39.2 0.1 copy.369
  40.4 0.1 copy.353
  40.5 0.3 multiply_subtract_fusion.2
  40.8 0.1 pad_maximum_fusion.1
  40.9 1.9 convolution_subtract_fusion.1
  42.8 5.3 %multiply_add_fusion = f32[8,4,128,128]{3,2,1,0:T(8,128)S(1)} fusion(f32[8,4,128,128]{3,2,1,0:T(8,128)} %copy-done.1, f32[8,4,4,128]{3,2,1,0:T(4,128)S(1)} %convolution_subtract_fusion.1, f32[8,4]{1,0:T(8,128)S(1)} %copy.352, bf16[8,4,512]{2,1,0:T(4,128)(2,1)S(1)} %copy-done.2, f32[8,4,4]{2,1,0:T(4,128)S(1)} %copy.353, f32[8,4,4]{2,1,0:T(4,128)S(1)} %add_rsqrt_fusion.2), kind=kOutput, calls=%fused_computation.8 | convolution fusion | flops 26263552 | bytes 4293760 | tf_op jit(solution)/shard_map/shpk,shpv->shkv/dot_general | solution.py:93
  48.1 10.1 %all-to-all-done = bf16[32,32,128]{2,1,0:T(8,128)(2,1)S(1)} async-done(((bf16[32,32,128]{2,1,0:T(8,128)(2,1)}), bf16[32,32,128]{2,1,0:T(8,128)(2,1)S(1)}, u32[]{:S(2)}, u32[]{:S(2)}) %all-to-all-start) | async-done | bytes 262176 | tf_op jit(solution)/shard_map/all_to_all | solution.py:124
  58.2 0.2 fusion.12
  58.4 0.2 convolution_multiply_fusion.3
  58.7 0.7 reduce_window_sum.17
  59.5 76.6 %all-gather.3.cloned.1.call-done = bf16[4096,2048]{1,0:T(8,128)(2,1)} async-done(((bf16[128,2048]{1,0:T(8,128)(2,1)}), bf16[4096,2048]{1,0:T(8,128)(2,1)}) %all-gather.3.cloned.1.call-update) | async-done | bytes 16777232 | tf_op jit(solution)/shard_map/all_gather | solution.py:18
  136.2 3.0 %fusion = f32[32,512]{1,0:T(8,128)S(1)} fusion(bf16[4096,2048]{1,0:T(8,128)(2,1)} %all-gather.3.cloned.1.call-done, f32[4096]{0:T(1024)S(1)} %convert_element_type.43, bf16[32,32,128]{2,1,0:T(8,128)(2,1)S(1)} %all-to-all-done), kind=kOutput, calls=%fused_computation | convolution fusion | flops 134610944 | bytes 4538368 | tf_op jit(solution)/shard_map/dot_general | solution.py:129
  139.2 3.0 %fusion.2 = f32[32,512]{1,0:T(8,128)S(1)} fusion(bf16[4096,2048]{1,0:T(8,128)(2,1)} %all-gather.3.cloned.1.call-done, f32[4096]{0:T(1024)S(1)} %convert_element_type.43, bf16[32,32,128]{2,1,0:T(8,128)(2,1)S(1)} %all-to-all-done), kind=kOutput, calls=%fused_computation.2 | convolution fusion | flops 134610944 | bytes 4538368 | tf_op jit(solution)/shard_map/dot_general | solution.py:129
  142.2 3.0 %fusion.4 = f32[32,512]{1,0:T(8,128)S(1)} fusion(bf16[4096,2048]{1,0:T(8,128)(2,1)} %all-gather.3.cloned.1.call-done, f32[4096]{0:T(1024)S(1)} %convert_element_type.43, bf16[32,32,128]{2,1,0:T(8,128)(2,1)S(1)} %all-to-all-done), kind=kOutput, calls=%fused_computation.4 | convolution fusion | flops 134610944 | bytes 4538368 | tf_op jit(solution)/shard_map/dot_general | solution.py:129
  145.2 3.0 %fusion.6 = f32[32,512]{1,0:T(8,128)S(1)} fusion(bf16[4096,2048]{1,0:T(8,128)(2,1)} %all-gather.3.cloned.1.call-done, f32[4096]{0:T(1024)S(1)} %convert_element_type.43, bf16[32,32,128]{2,1,0:T(8,128)(2,1)S(1)} %all-to-all-done), kind=kOutput, calls=%fused_computation.6 | convolution fusion | flops 134610944 | bytes 4538368 | tf_op jit(solution)/shard_map/dot_general | solution.py:129
  148.4 0.1 fusion.24
  148.5 0.1 fusion.32
  148.7 0.1 fusion.38
  148.9 0.4 convolution_multiply_fusion.1
  149.3 0.4 fusion.9
  149.8 0.2 fusion.78
  151.1 0.3 multiply_subtract_fusion
  151.4 0.1 pad_maximum_fusion.2
  151.6 1.9 convolution_subtract_fusion
  153.4 1.9 fusion.34
  155.3 0.4 fusion.80
  155.7 0.1 fusion.20
  155.8 0.1 copy.393
  155.9 0.1 copy.394
  156.2 26.2 %all_gather.10 = bf16[16,32,512]{2,1,0:T(8,128)(2,1)} all-gather(bf16[1,32,512]{2,1,0:T(8,128)(2,1)S(1)} %convert_element_type.48), channel_id=1, replica_groups=mesh['grp'=2,'kv_0'=16,'kv_1'=2,'tp'=4] {'kv_0'}, dimensions={0}, use_global_device_ids=true | all-gather | bytes 557056 | tf_op jit(solution)/shard_map/all_gather | solution.py:30
  182.5 25.5 %all-gather.5.cloned.1.call-done = bf16[32,32,512]{2,1,0:T(8,128)(2,1)} async-done(((bf16[16,32,512]{2,1,0:T(8,128)(2,1)}), bf16[32,32,512]{2,1,0:T(8,128)(2,1)}) %all-gather.5.cloned.1.call-update) | async-done | bytes 1048592 | tf_op jit(solution)/shard_map/all_gather | solution.py:30
  208.0 1.3 copy.398
  209.3 0.4 fusion.81
  209.7 1.5 broadcast_in_dim.79
  211.2 4.5 %all-to-all-start.1 = ((f32[4,1024,128]{2,1,0:T(8,128)}), f32[4,1024,128]{2,1,0:T(8,128)}, u32[]{:S(2)}, u32[]{:S(2)}) async-start(f32[4,1024,128]{2,1,0:T(8,128)} %broadcast_in_dim.79), calls=%async_computation.1 | async-start | bytes 4194304 | tf_op jit(solution)/shard_map/all_to_all | solution.py:43
  215.7 1.9 reshape.149
  217.6 24.3 %all-to-all-done.1 = f32[4,1024,128]{2,1,0:T(8,128)} async-done(((f32[4,1024,128]{2,1,0:T(8,128)}), f32[4,1024,128]{2,1,0:T(8,128)}, u32[]{:S(2)}, u32[]{:S(2)}) %all-to-all-start.1) | async-done | bytes 2097184 | tf_op jit(solution)/shard_map/all_to_all | solution.py:43
  241.9 2.5 reduce_sum.59
  (83 shorter events, 3.4 us)
Async XLA Ops:
  7.2 202.1 %copy-start = (bf16[512,128]{1,0:T(8,128)(2,1)S(1)}, bf16[512,128]{1,0:T(8,128)(2,1)}, u32[]{:S(2)}) copy-start(bf16[512,128]{1,0:T(8,128)(2,1)} %param.27) | copy-start | bytes 393220
  7.2 27.8 %copy-start.9 = (s32[8]{0:T(128)S(1)}, s32[8]{0:T(128)}, u32[]{:S(2)}) copy-start(s32[8]{0:T(128)} %param.33) | copy-start | bytes 100
  7.2 27.8 %copy-start.5 = (f32[8,4,4]{0,2,1:T(4,128)S(1)}, f32[8,4,4]{0,2,1:T(4,128)}, u32[]{:S(2)}) copy-start(f32[8,4,4]{0,2,1:T(4,128)} %param.31) | copy-start | bytes 1540
  7.2 27.9 %copy-start.6 = (f32[8,4,4]{0,2,1:T(4,128)S(1)}, f32[8,4,4]{0,2,1:T(4,128)}, u32[]{:S(2)}) copy-start(f32[8,4,4]{0,2,1:T(4,128)} %param.32) | copy-start | bytes 1540
  7.2 28.2 %copy-start.2 = (bf16[8,4,512]{2,1,0:T(4,128)(2,1)S(1)}, bf16[8,4,512]{2,1,0:T(4,128)(2,1)}, u32[]{:S(2)}) copy-start(bf16[8,4,512]{2,1,0:T(4,128)(2,1)} %param.29) | copy-start | bytes 98308
  7.2 28.8 %copy-start.3 = (bf16[8,4,512]{2,1,0:T(4,128)(2,1)S(1)}, bf16[8,4,512]{2,1,0:T(4,128)(2,1)}, u32[]{:S(2)}) copy-start(bf16[8,4,512]{2,1,0:T(4,128)(2,1)} %param.30) | copy-start | bytes 98308
  7.2 29.2 %copy-start.4 = (bf16[4096]{0:T(1024)(128)(2,1)S(1)}, bf16[4096]{0:T(1024)(128)(2,1)}, u32[]{:S(2)}) copy-start(bf16[4096]{0:T(1024)(128)(2,1)} %param.18) | copy-start | bytes 24580
  7.3 29.2 %copy-start.10 = (bf16[128]{0:T(256)(128)(2,1)S(1)}, bf16[128]{0:T(256)(128)(2,1)}, u32[]{:S(2)}) copy-start(bf16[128]{0:T(256)(128)(2,1)} %param.26) | copy-start | bytes 772
  7.3 29.2 %copy-start.11 = (f32[4]{0:T(128)S(1)}, f32[4]{0:T(128)}, u32[]{:S(2)}) copy-start(f32[4]{0:T(128)} %param.25) | copy-start | bytes 52
  7.3 128.9 %all-gather.3.cloned.1.call-start = ((), (), s32[]{:S(2)}) async-start(), calls=%async_computation.2 | async-start | bytes 17301504 | tf_op jit(solution)/shard_map/all_gather | solution.py:18
  9.4 48.8 %all-to-all-start = ((bf16[32,32,128]{2,1,0:T(8,128)(2,1)}), bf16[32,32,128]{2,1,0:T(8,128)(2,1)S(1)}, u32[]{:S(2)}, u32[]{:S(2)}) async-start(bf16[32,32,128]{2,1,0:T(8,128)(2,1)} %bitcast.155), calls=%async_computation | async-start | bytes 524288 | tf_op jit(solution)/shard_map/all_to_all | solution.py:124
  34.9 173.1 %all-gather.5.cloned.1.call-start = ((), (), s32[]{:S(2)}) async-start(), calls=%async_computation.3 | async-start | bytes 1572864 | tf_op jit(solution)/shard_map/all_gather | solution.py:30
  39.2 1.8 copy-start.1
  42.8 15.6 %copy-start.7 = (bf16[4096,4]{0,1:T(4,128)(2,1)S(1)}, bf16[4096,4]{0,1:T(4,128)(2,1)}, u32[]{:S(2)}) copy-start(bf16[4096,4]{0,1:T(4,128)(2,1)} %param.24) | copy-start | bytes 98308
  42.8 15.6 %copy-start.8 = (bf16[4096,4]{0,1:T(4,128)(2,1)S(1)}, bf16[4096,4]{0,1:T(4,128)(2,1)}, u32[]{:S(2)}) copy-start(bf16[4096,4]{0,1:T(4,128)(2,1)} %param.23) | copy-start | bytes 98308
  211.2 30.7 %all-to-all-start.1 = ((f32[4,1024,128]{2,1,0:T(8,128)}), f32[4,1024,128]{2,1,0:T(8,128)}, u32[]{:S(2)}, u32[]{:S(2)}) async-start(f32[4,1024,128]{2,1,0:T(8,128)} %broadcast_in_dim.79), calls=%async_computation.1 | async-start | bytes 4194304 | tf_op jit(solution)/shard_map/all_to_all | solution.py:43
Sparse Core Ops, SparseCore 0:
  10.0 126.1 all-gather.2
  182.6 25.3 all-gather.4
where the time goes:
time: 252 us; the launch traced here: 251 us
  waiting for transfers between devices  137 us (54%)
  starting transfers between devices  30.2 us (12%)
  blocking collectives  26.2 us (10%)
  matrix products  25.2 us (10%)
  between operations  14.6 us (6%)
  local copies, waits for them, and re-layouts  11 us (4%)
  other arithmetic  7.45 us (3%)
    all_gather x1, waiting for transfers between devices, side_by_side(): lax.all_gather(both, axis, axis=dim, tiled=True)  76.6 us
    all_gather x1, blocking collectives, gather_in_order(): tiles = lax.all_gather(tiles, axes[k], axis=0, tiled=True)  26.2 us
    all_to_all x1, starting transfers between devices, per_device(): lax.all_to_all(hidden, KV, split_axis=0, concat_axis=1, tiled=True)  25.5 us
    all_gather x1, waiting for transfers between devices, gather_in_order(): tiles = lax.all_gather(tiles, axes[k], axis=0, tiled=True)  25.5 us
    all_to_all x1, waiting for transfers between devices, from_everyone(): return lax.all_to_all(copies, axis, split_axis=0, concat_axis=0, tiled=True)  24.3 us
    dot_general x4, matrix products, per_device(): jnp.dot(scaled, piece, preferred_element_type=jnp.float32)  12 us
    all_to_all x1, waiting for transfers between devices, per_device(): lax.all_to_all(hidden, KV, split_axis=0, concat_axis=1, tiled=True)  10.1 us
    dot_general x1, matrix products, delta_block(): jnp.einsum('shpk,shpv->shkv', keys * jnp.exp(final - totals)[..., None],...  5.32 us
  transfers between devices with their start and end apart: 4, of which 4 were waited for; matrix products, arithmetic and copies ran while one was open for 6% of the time, Pallas kernels for 0%

commit v1 on v0

--- a/solution.py
+++ b/solution.py
@@ -27,7 +27,9 @@
 def gather_in_order(value, axes, turns):
     tiles = value[None]
     for k in turns:
-        tiles = lax.all_gather(tiles, axes[k], axis=0, tiled=True)
+        tiles = jnp.concatenate(
+            lax.all_to_all(jnp.stack([tiles] * lax.axis_size(axes[k])), axes[k], 0, 0), axis=0
+        )
     block = [lax.axis_size(axes[k]) for k in reversed(turns)]
     tiles = tiles.reshape(*block, *value.shape)
     turned = sorted(range(len(turns)), key=lambda place: turns[len(turns) - 1 - place])

time: 252 us -> 242 us (0.960)
  waiting for transfers between devices: 137 us -> 111 us
  blocking collectives: 26.2 us -> 42.7 us
    all_to_all x0 -> x2, blocking collectives: none -> 42.7 us  [gather_in_order(): lax.all_to_all(jnp.stack([tiles] * lax.axis_size(axes[k])), axes[k], 0, 0)]
    all_gather x1 -> x0, blocking collectives: 26.2 us -> none  [gather_in_order(): tiles = lax.all_gather(tiles, axes[k], axis=0, tiled=True)]
    all_gather x1 -> x0, waiting for transfers between devices: 25.5 us -> none  [gather_in_order(): tiles = lax.all_gather(tiles, axes[k], axis=0, tiled=True)]
  transfers between devices with their start and end apart: 4 -> 3, of which waited for: 4 -> 3; matrix products, arithmetic and copies ran while one was open for 6% -> 7% of each run, Pallas kernels for 0% -> 0%
where the time goes in v1:
time: 242 us; the launch traced here: 241 us
  waiting for transfers between devices  111 us (46%)
  blocking collectives  42.7 us (18%)
  starting transfers between devices  30.1 us (12%)
  matrix products  25.2 us (10%)
  between operations  14.6 us (6%)
  local copies, waits for them, and re-layouts  9.83 us (4%)
  other arithmetic  7.53 us (3%)
    all_gather x1, waiting for transfers between devices, side_by_side(): lax.all_gather(both, axis, axis=dim, tiled=True)  76.7 us
    all_to_all x2, blocking collectives, gather_in_order(): lax.all_to_all(jnp.stack([tiles] * lax.axis_size(axes[k])), axes[k], 0, 0)  42.7 us
    all_to_all x1, starting transfers between devices, per_device(): lax.all_to_all(hidden, KV, split_axis=0, concat_axis=1, tiled=True)  25.5 us
    all_to_all x1, waiting for transfers between devices, from_everyone(): return lax.all_to_all(copies, axis, split_axis=0, concat_axis=0, tiled=True)  24.2 us
    dot_general x4, matrix products, per_device(): jnp.dot(scaled, piece, preferred_element_type=jnp.float32)  12 us
    all_to_all x1, waiting for transfers between devices, per_device(): lax.all_to_all(hidden, KV, split_axis=0, concat_axis=1, tiled=True)  10.1 us
    dot_general x1, matrix products, delta_block(): jnp.einsum('shpk,shpv->shkv', keys * jnp.exp(final - totals)[..., None],...  5.32 us
  transfers between devices with their start and end apart: 3, of which 3 were waited for; matrix products, arithmetic and copies ran while one was open for 7% of the time, Pallas kernels for 0%

profile of v1, /device:TPU:33, one launch (start us, length us, event | category | flops | bytes accessed | tf_op | source)
XLA Modules:
  0.0 241.0 jit_solution(6642423522985516015)
XLA Ops:
  7.3 2.0 pad_maximum_fusion.1
  9.4 25.5 %all-to-all-start = ((bf16[32,32,128]{2,1,0:T(8,128)(2,1)}), bf16[32,32,128]{2,1,0:T(8,128)(2,1)S(1)}, u32[]{:S(2)}, u32[]{:S(2)}) async-start(bf16[32,32,128]{2,1,0:T(8,128)(2,1)} %bitcast.160), calls=%async_computation | async-start | bytes 524288 | tf_op jit(solution)/shard_map/all_to_all | solution.py:126
  35.0 0.1 copy.311
  35.1 0.1 copy.308
  35.2 0.1 copy.309
  35.3 0.1 fusion.31
  35.5 0.4 fusion.11
  36.0 0.2 fusion.19
  36.2 0.2 fusion.79
  36.4 2.7 %reshape.136 = f32[8,4,128,128]{3,2,1,0:T(8,128)S(1)} reshape(f32[8,4,16384]{2,1,0:T(4,128)} %param.28) | data formatting | bytes 4194304 | tf_op jit(solution)/shard_map/reshape | solution.py:168
  39.1 0.1 copy.323
  40.3 0.1 copy.307
  40.4 0.3 multiply_subtract_fusion.2
  40.7 0.1 pad_maximum_fusion.2
  40.8 1.9 convolution_subtract_fusion.1
  42.7 5.3 %multiply_add_fusion = f32[8,4,128,128]{3,2,1,0:T(8,128)S(1)} fusion(f32[8,4,128,128]{3,2,1,0:T(8,128)} %copy-done.1, f32[8,4,4,128]{3,2,1,0:T(4,128)S(1)} %convolution_subtract_fusion.1, f32[8,4]{1,0:T(8,128)S(1)} %copy.306, bf16[8,4,512]{2,1,0:T(4,128)(2,1)S(1)} %copy-done.2, f32[8,4,4]{2,1,0:T(4,128)S(1)} %copy.307, f32[8,4,4]{2,1,0:T(4,128)S(1)} %add_rsqrt_fusion.2), kind=kOutput, calls=%fused_computation.8 | convolution fusion | flops 26263552 | bytes 4293760 | tf_op jit(solution)/shard_map/shpk,shpv->shkv/dot_general | solution.py:95
  48.0 10.1 %all-to-all-done = bf16[32,32,128]{2,1,0:T(8,128)(2,1)S(1)} async-done(((bf16[32,32,128]{2,1,0:T(8,128)(2,1)}), bf16[32,32,128]{2,1,0:T(8,128)(2,1)S(1)}, u32[]{:S(2)}, u32[]{:S(2)}) %all-to-all-start) | async-done | bytes 262176 | tf_op jit(solution)/shard_map/all_to_all | solution.py:126
  58.2 0.2 fusion.12
  58.4 0.2 convolution_multiply_fusion.3
  58.7 0.7 reduce_window_sum.17
  59.5 76.7 %all-gather.2.cloned.1.call-done = bf16[4096,2048]{1,0:T(8,128)(2,1)} async-done(((bf16[128,2048]{1,0:T(8,128)(2,1)}), bf16[4096,2048]{1,0:T(8,128)(2,1)}) %all-gather.2.cloned.1.call-update) | async-done | bytes 16777232 | tf_op jit(solution)/shard_map/all_gather | solution.py:18
  136.2 3.0 %fusion = f32[32,512]{1,0:T(8,128)S(1)} fusion(bf16[4096,2048]{1,0:T(8,128)(2,1)} %all-gather.2.cloned.1.call-done, f32[4096]{0:T(1024)S(1)} %convert_element_type.41, bf16[32,32,128]{2,1,0:T(8,128)(2,1)S(1)} %all-to-all-done), kind=kOutput, calls=%fused_computation | convolution fusion | flops 134610944 | bytes 4538368 | tf_op jit(solution)/shard_map/dot_general | solution.py:131
  139.2 3.0 %fusion.2 = f32[32,512]{1,0:T(8,128)S(1)} fusion(bf16[4096,2048]{1,0:T(8,128)(2,1)} %all-gather.2.cloned.1.call-done, f32[4096]{0:T(1024)S(1)} %convert_element_type.41, bf16[32,32,128]{2,1,0:T(8,128)(2,1)S(1)} %all-to-all-done), kind=kOutput, calls=%fused_computation.2 | convolution fusion | flops 134610944 | bytes 4538368 | tf_op jit(solution)/shard_map/dot_general | solution.py:131
  142.2 3.0 %fusion.4 = f32[32,512]{1,0:T(8,128)S(1)} fusion(bf16[4096,2048]{1,0:T(8,128)(2,1)} %all-gather.2.cloned.1.call-done, f32[4096]{0:T(1024)S(1)} %convert_element_type.41, bf16[32,32,128]{2,1,0:T(8,128)(2,1)S(1)} %all-to-all-done), kind=kOutput, calls=%fused_computation.4 | convolution fusion | flops 134610944 | bytes 4538368 | tf_op jit(solution)/shard_map/dot_general | solution.py:131
  145.2 3.0 %fusion.6 = f32[32,512]{1,0:T(8,128)S(1)} fusion(bf16[4096,2048]{1,0:T(8,128)(2,1)} %all-gather.2.cloned.1.call-done, f32[4096]{0:T(1024)S(1)} %convert_element_type.41, bf16[32,32,128]{2,1,0:T(8,128)(2,1)S(1)} %all-to-all-done), kind=kOutput, calls=%fused_computation.6 | convolution fusion | flops 134610944 | bytes 4538368 | tf_op jit(solution)/shard_map/dot_general | solution.py:131
  148.4 0.1 fusion.24
  148.5 0.1 fusion.32
  148.7 0.1 fusion.38
  148.9 0.4 convolution_multiply_fusion.1
  149.3 0.4 fusion.9
  149.8 0.2 fusion.78
  150.0 0.1 copy.342
  151.1 0.3 multiply_subtract_fusion
  151.4 0.1 pad_maximum_fusion.3
  151.6 1.9 convolution_subtract_fusion
  153.4 1.9 fusion.34
  155.3 0.4 fusion.80
  155.7 0.1 fusion.20
  155.8 0.1 copy.347
  155.9 0.1 copy.348
  156.2 31.4 %all_to_all.28 = bf16[16,1,32,512]{3,2,1,0:T(8,128)(2,1)S(1)} all-to-all(bf16[16,1,32,512]{3,2,1,0:T(8,128)(2,1)S(1)} %stack.20), channel_id=1, replica_groups=mesh['grp'=2,'kv_0'=16,'kv_1'=2,'tp'=4] {'kv_0'}, dimensions={0} | all-to-all | bytes 1048576 | tf_op jit(solution)/shard_map/all_to_all | solution.py:31
  187.7 11.4 %all_to_all.29 = bf16[2,16,32,512]{3,2,1,0:T(8,128)(2,1)S(1)} all-to-all(bf16[2,16,32,512]{3,2,1,0:T(8,128)(2,1)S(1)} %pad_maximum_fusion), channel_id=1, replica_groups=mesh['grp'=2,'kv_0'=16,'kv_1'=2,'tp'=4] {'kv_1'}, dimensions={0} | all-to-all | bytes 2097152 | tf_op jit(solution)/shard_map/all_to_all | solution.py:31
  199.2 0.4 fusion.81
  199.6 1.4 broadcast_in_dim.78
  201.0 4.5 %all-to-all-start.3 = ((f32[4,1024,128]{2,1,0:T(8,128)}), f32[4,1024,128]{2,1,0:T(8,128)}, u32[]{:S(2)}, u32[]{:S(2)}) async-start(f32[4,1024,128]{2,1,0:T(8,128)} %broadcast_in_dim.78), calls=%async_computation.3 | async-start | bytes 4194304 | tf_op jit(solution)/shard_map/all_to_all | solution.py:45
  205.6 1.9 reshape.143
  207.4 24.2 %all-to-all-done.3 = f32[4,1024,128]{2,1,0:T(8,128)} async-done(((f32[4,1024,128]{2,1,0:T(8,128)}), f32[4,1024,128]{2,1,0:T(8,128)}, u32[]{:S(2)}, u32[]{:S(2)}) %all-to-all-start.3) | async-done | bytes 2097184 | tf_op jit(solution)/shard_map/all_to_all | solution.py:45
  231.6 2.5 %reduce_sum.59 = bf16[1024,128]{1,0:T(8,128)(2,1)} reduce(f32[4,1024,128]{2,1,0:T(8,128)} %all-to-all-done.3, f32[]{:T(128)} %constant.18.clone.1), dimensions={0}, to_apply=%region_7.8 | reduce | flops 393216 | bytes 2359300 | tf_op jit(solution)/shard_map/reduce_sum | solution.py:49
  (83 shorter events, 3.4 us)
Async XLA Ops:
  7.2 192.0 %copy-start = (bf16[512,128]{1,0:T(8,128)(2,1)S(1)}, bf16[512,128]{1,0:T(8,128)(2,1)}, u32[]{:S(2)}) copy-start(bf16[512,128]{1,0:T(8,128)(2,1)} %param.27) | copy-start | bytes 393220
  7.2 27.7 %copy-start.9 = (s32[8]{0:T(128)S(1)}, s32[8]{0:T(128)}, u32[]{:S(2)}) copy-start(s32[8]{0:T(128)} %param.33) | copy-start | bytes 100
  7.2 27.7 %copy-start.5 = (f32[8,4,4]{0,2,1:T(4,128)S(1)}, f32[8,4,4]{0,2,1:T(4,128)}, u32[]{:S(2)}) copy-start(f32[8,4,4]{0,2,1:T(4,128)} %param.31) | copy-start | bytes 1540
  7.2 27.8 %copy-start.6 = (f32[8,4,4]{0,2,1:T(4,128)S(1)}, f32[8,4,4]{0,2,1:T(4,128)}, u32[]{:S(2)}) copy-start(f32[8,4,4]{0,2,1:T(4,128)} %param.32) | copy-start | bytes 1540
  7.2 28.1 %copy-start.2 = (bf16[8,4,512]{2,1,0:T(4,128)(2,1)S(1)}, bf16[8,4,512]{2,1,0:T(4,128)(2,1)}, u32[]{:S(2)}) copy-start(bf16[8,4,512]{2,1,0:T(4,128)(2,1)} %param.29) | copy-start | bytes 98308
  7.2 28.7 %copy-start.3 = (bf16[8,4,512]{2,1,0:T(4,128)(2,1)S(1)}, bf16[8,4,512]{2,1,0:T(4,128)(2,1)}, u32[]{:S(2)}) copy-start(bf16[8,4,512]{2,1,0:T(4,128)(2,1)} %param.30) | copy-start | bytes 98308
  7.2 29.1 %copy-start.4 = (bf16[4096]{0:T(1024)(128)(2,1)S(1)}, bf16[4096]{0:T(1024)(128)(2,1)}, u32[]{:S(2)}) copy-start(bf16[4096]{0:T(1024)(128)(2,1)} %param.18) | copy-start | bytes 24580
  7.3 29.1 %copy-start.10 = (bf16[128]{0:T(256)(128)(2,1)S(1)}, bf16[128]{0:T(256)(128)(2,1)}, u32[]{:S(2)}) copy-start(bf16[128]{0:T(256)(128)(2,1)} %param.26) | copy-start | bytes 772
  7.3 29.1 %copy-start.11 = (f32[4]{0:T(128)S(1)}, f32[4]{0:T(128)}, u32[]{:S(2)}) copy-start(f32[4]{0:T(128)} %param.25) | copy-start | bytes 52
  7.3 128.9 %all-gather.2.cloned.1.call-start = ((), (), s32[]{:S(2)}) async-start(), calls=%async_computation.4 | async-start | bytes 17301504 | tf_op jit(solution)/shard_map/all_gather | solution.py:18
  9.4 48.8 %all-to-all-start = ((bf16[32,32,128]{2,1,0:T(8,128)(2,1)}), bf16[32,32,128]{2,1,0:T(8,128)(2,1)S(1)}, u32[]{:S(2)}, u32[]{:S(2)}) async-start(bf16[32,32,128]{2,1,0:T(8,128)(2,1)} %bitcast.160), calls=%async_computation | async-start | bytes 524288 | tf_op jit(solution)/shard_map/all_to_all | solution.py:126
  39.1 1.8 copy-start.1
  42.7 15.7 %copy-start.7 = (bf16[4096,4]{0,1:T(4,128)(2,1)S(1)}, bf16[4096,4]{0,1:T(4,128)(2,1)}, u32[]{:S(2)}) copy-start(bf16[4096,4]{0,1:T(4,128)(2,1)} %param.24) | copy-start | bytes 98308
  42.7 15.7 %copy-start.8 = (bf16[4096,4]{0,1:T(4,128)(2,1)S(1)}, bf16[4096,4]{0,1:T(4,128)(2,1)}, u32[]{:S(2)}) copy-start(bf16[4096,4]{0,1:T(4,128)(2,1)} %param.23) | copy-start | bytes 98308
  201.0 30.6 %all-to-all-start.3 = ((f32[4,1024,128]{2,1,0:T(8,128)}), f32[4,1024,128]{2,1,0:T(8,128)}, u32[]{:S(2)}, u32[]{:S(2)}) async-start(f32[4,1024,128]{2,1,0:T(8,128)} %broadcast_in_dim.78), calls=%async_computation.3 | async-start | bytes 4194304 | tf_op jit(solution)/shard_map/all_to_all | solution.py:45
Sparse Core Ops, SparseCore 0:
  10.0 126.1 all-gather.1
